TPU v7x, 32 devices: a whole 2x2x4 slice. The times are simulated.
32 devices in a mesh: sp: 16 (over z, y, core), tp: 2 (over x).
Axes of the slice: x: 2, y: 2, z: 4, core: 2. Of those that a mesh axis runs over, the one named last changes fastest.
Arguments:
- residual: bfloat16 [2048, 2048], P(('sp', 'tp')), may hold values from -6 to 6
- forget_forward: bfloat16 [2048, 1024], P('sp', 'tp'), may hold values from -5.5 to 5.5
- forget_backward: bfloat16 [2048, 1024], P('sp', 'tp'), may hold values from -5.5 to 5.5
- value_written: bfloat16 [2048, 1024], P('sp', 'tp'), may hold values from -6 to 6
- query_logits: bfloat16 [2048, 1024], P('sp', 'tp'), may hold values from -6 to 6
- output_gate_logits: bfloat16 [2048, 1024], P('sp', 'tp'), may hold values from -6 to 6
- forget_minimum: float32 [2, 1024], P(None, 'tp'), may hold values from 0.88 to 1
- extra_log_rate: float32 [2, 2048, 8], P(None, 'sp', 'tp'), may hold values from -0.7 to 0
- head_norm_scale: float32 [128], replicated, may hold values from 0.1 to 1.9
- output_matrix: bfloat16 [1024, 2048], P(None, 'sp'), may hold values from -0.1875 to 0.1875
- prenorm_scale: float32 [2048], replicated, may hold values from 0.1 to 1.9
- gate_up_matrix: bfloat16 [2048, 5632], P('sp', 'tp'), may hold values from -0.125 to 0.125
- value_up_matrix: bfloat16 [2048, 5632], P('sp', 'tp'), may hold values from -0.125 to 0.125
- gate_taps: float32 [3, 5632], P(None, 'tp'), may hold values from -3.5 to 3.5
- value_taps: float32 [3, 5632], P(None, 'tp'), may hold values from -3.5 to 3.5
- down_matrix: bfloat16 [5632, 2048], P('tp', 'sp'), may hold values from -0.078125 to 0.078125
Outputs:
- layer_out: bfloat16 [2048, 2048], P(('sp', 'tp'))
All inputs are finite; a program needn't handle non-finite values.
Results may differ from a plain program's by a relative error of at most 0.012.
Values may be sent and summed in bfloat16 or wider, within the bound.
No kernel may reach another device: no remote copies, remote signals or barrier semaphores. Data moves between devices by JAX's collectives and lax.ppermute only.
A program may use at most 128 MiB of HBM per device.

v0:
```python
import jax
import jax.numpy as jnp
from jax import lax
from jax.sharding import PartitionSpec as P

HEAD_WIDTH = 128
BLOCK = 64


EPSILON = 1e-06


def carried_in(array, axis, combine, identity, reverse):
    size, position = (lax.axis_size(axis), lax.axis_index(axis))
    everything = jax.tree.map(
        lambda part, kind: lax.all_gather(part.astype(kind), axis),
        array,
        (jnp.bfloat16, jnp.bfloat16),
    )
    start = jax.tree.map(
        lambda part, zero: jnp.broadcast_to(jnp.asarray(zero, part.dtype), part.shape),
        array,
        identity,
    )

    def hop(k, before):
        at = size - 1 - k if reverse else k
        reached = at > position if reverse else at < position
        new = combine(
            before, jax.tree.map(lambda part, own: part[at].astype(own.dtype), everything, array)
        )
        return jax.tree.map(lambda a, b: jnp.where(reached, a, b), new, before)

    return lax.fori_loop(0, size, hop, start)


def extended(array, sides, width):
    for axis, dim in sides:
        size, length = (lax.axis_size(axis), array.shape[dim])
        up = [(i, (i + 1) % size) for i in range(size - 1)]
        down = [(j, i) for i, j in up]
        last = lax.slice_in_dim(array, length - width, length, axis=dim)
        initial = lax.slice_in_dim(array, 0, width, axis=dim)
        before = lax.ppermute(last, axis, up)
        after = lax.ppermute(initial, axis, down)
        array = jnp.concatenate([before, array, after], axis=dim)
    return array


def rms_scale(array):
    return array * lax.rsqrt(jnp.mean(array * array, axis=-1, keepdims=True) + EPSILON)


def forget_factors(forget_logits, forget_floor, extra_decay):
    unbounded_gate = forget_logits.astype(jnp.float32)
    log_forget_gate = jnp.log(
        forget_floor + (1.0 - forget_floor) * jax.nn.sigmoid(unbounded_gate)
    ) + jnp.repeat(extra_decay, HEAD_WIDTH, axis=1)
    key_in = (1.0 - forget_floor) * jax.nn.sigmoid(-unbounded_gate)
    shape = (unbounded_gate.shape[0], unbounded_gate.shape[1] // HEAD_WIDTH, HEAD_WIDTH)
    return (log_forget_gate.reshape(shape), key_in.reshape(shape))


def block_scan(log_forget_gate, key_in, values, queries):
    length, heads, depth = log_forget_gate.shape
    width = values.shape[2]
    blocks = length // BLOCK
    highest = lax.Precision.HIGHEST
    lower = jnp.tril(jnp.ones((BLOCK, BLOCK), dtype=bool))[:, :, None, None]

    def split(array):
        return array.reshape(blocks, BLOCK, heads, array.shape[2])

    def advance(carry, pieces):
        state, carried = carry
        log_part, key_part, value_part, query_part = pieces
        running = jnp.cumsum(log_part, axis=0)
        block_total = running[-1]
        query_carry = query_part * jnp.exp(carried[None] + running)
        from_state = jnp.einsum(
            "chd,hde->che", query_part * jnp.exp(running), state, precision=highest
        )
        gaps = jnp.where(lower, running[:, None] - running[None, :], -1e30)
        scores = jnp.einsum(
            "ihd,jhd,ijhd->hij", query_part, key_part, jnp.exp(gaps), precision=highest
        )
        inside = jnp.einsum("hij,jhe->ihe", scores, value_part, precision=highest)
        fresh = jnp.einsum(
            "chd,che->hde",
            key_part * jnp.exp(block_total[None] - running),
            value_part,
            precision=highest,
        )
        state = jnp.exp(block_total)[:, :, None] * state + fresh
        return ((state, carried + block_total), (from_state + inside, query_carry))

    start = (jnp.zeros((heads, depth, width), jnp.float32), jnp.zeros((heads, depth), jnp.float32))
    (state, carried), (outputs, query_carry) = lax.scan(
        advance, start, (split(log_forget_gate), split(key_in), split(values), split(queries))
    )
    return (
        state,
        carried,
        outputs.reshape(length, heads, width),
        query_carry.reshape(length, heads, depth),
    )


def link_states(earlier, later):
    return (earlier[0] + later[0], jnp.exp(later[0])[:, :, None] * earlier[1] + later[1])


def on_device(
    residual,
    forget_forward,
    forget_backward,
    value_written,
    query_logits,
    output_gate_logits,
    forget_minimum,
    extra_log_rate,
    head_norm_scale,
    output_matrix,
    prenorm_scale,
    gate_up_matrix,
    value_up_matrix,
    gate_taps,
    value_taps,
    down_matrix,
):
    highest = lax.Precision.HIGHEST
    length = value_written.shape[0]
    shape = (length, value_written.shape[1] // HEAD_WIDTH, HEAD_WIDTH)
    gate_full, value_full, down_full, out_full = (
        lax.all_gather(gate_up_matrix, "sp", axis=0, tiled=True),
        lax.all_gather(value_up_matrix, "sp", axis=0, tiled=True),
        lax.all_gather(down_matrix, "sp", axis=1, tiled=True),
        lax.all_gather(output_matrix, "sp", axis=1, tiled=True),
    )
    values = value_written.astype(jnp.float32).reshape(shape)
    queries = jax.nn.silu(query_logits.astype(jnp.float32)).reshape(shape)
    log_decay_forward, key_forward = forget_factors(
        forget_forward, forget_minimum[0], extra_log_rate[0]
    )
    state, carried, forward, carry_fwd = block_scan(log_decay_forward, key_forward, values, queries)
    empty = (jnp.zeros_like(carried), jnp.zeros_like(state))
    entering = carried_in((carried, state), "sp", link_states, empty, False)
    forward = forward + jnp.einsum("thd,hde->the", carry_fwd, entering[1], precision=highest)
    log_decay_backward, key_backward = forget_factors(
        forget_backward, forget_minimum[1], extra_log_rate[1]
    )
    state, carried, backward, carry_bwd = block_scan(
        log_decay_backward[::-1], key_backward[::-1], values[::-1], queries[::-1]
    )
    entering = carried_in((carried, state), "sp", link_states, empty, True)
    backward = (backward + jnp.einsum("thd,hde->the", carry_bwd, entering[1], precision=highest))[
        ::-1
    ]
    gated = (
        rms_scale(forward + backward)
        * head_norm_scale
        * jax.nn.silu(output_gate_logits.astype(jnp.float32)).reshape(shape)
    )
    mixed_in = gated.reshape(length, shape[1] * HEAD_WIDTH).astype(jnp.bfloat16)
    token_rows = lax.all_to_all(mixed_in, "tp", split_axis=0, concat_axis=1, tiled=True)
    mixed = jnp.dot(token_rows, out_full, preferred_element_type=jnp.float32)
    own_after = residual.astype(jnp.float32) + mixed
    normed = (rms_scale(own_after) * prenorm_scale).astype(jnp.bfloat16)
    normed_all = lax.all_gather(normed, "tp", axis=0, tiled=True)
    gate_up = jnp.dot(normed_all, gate_full, preferred_element_type=jnp.float32)
    value_up = jnp.dot(normed_all, value_full, preferred_element_type=jnp.float32)
    upward = jnp.concatenate([gate_up.astype(jnp.bfloat16), value_up.astype(jnp.bfloat16)], axis=1)
    padded = extended(upward, (("sp", 0),), 1)
    kernel = jnp.concatenate([gate_taps, value_taps], axis=1)
    convolved = (
        padded[:length] * kernel[0] + padded[1 : length + 1] * kernel[1] + padded[2:] * kernel[2]
    )
    hidden_width = gate_up_matrix.shape[1]
    hidden = (jax.nn.silu(convolved[:, :hidden_width]) * convolved[:, hidden_width:]).astype(
        jnp.bfloat16
    )
    terms = jnp.dot(hidden, down_full, preferred_element_type=jnp.float32)
    down_sum = lax.psum_scatter(
        terms.astype(jnp.bfloat16), "tp", scatter_dimension=0, tiled=True
    ).astype(jnp.float32)
    return (own_after + down_sum).astype(jnp.bfloat16)


def solution(mesh):
    return jax.shard_map(
        on_device,
        mesh=mesh,
        in_specs=(
            P(("sp", "tp"), None),
            P("sp", "tp"),
            P("sp", "tp"),
            P("sp", "tp"),
            P("sp", "tp"),
            P("sp", "tp"),
            P(None, "tp"),
            P(None, "sp", "tp"),
            P(),
            P(None, "sp"),
            P(),
            P("sp", "tp"),
            P("sp", "tp"),
            P(None, "tp"),
            P(None, "tp"),
            P("tp", "sp"),
        ),
        out_specs=P(("sp", "tp"), None),
        check_vma=False,
    )
```

profile of v0, /device:TPU:24, one launch (start us, length us, event | category | flops | bytes accessed | tf_op | source)
XLA Modules:
  0.0 495.1 jit_solution(2763869349589642076)
XLA Ops:
  10.7 29.9 %while.66 = (s32[]{:T(128)}, f32[4,128,128]{2,1,0:T(8,128)S(1)}, f32[4,128]{1,0:T(4,128)S(1)}, f32[2,64,4,128]{3,1,0,2:T(8,128)S(1)}, f32[2,64,4,128]{3,2,1,0:T(...) while((s32[]{:T(128)}, f32[4,128,128]{2,1,0:T(8,128)S(1)}, ...), condition=%wide.region_7.8_spmd.clone, body=%wide.region_5.7_spmd.clone.sunk | while | flops 138826752 | bytes 21328020 | solution.py:98
  11.0 5.9 %exponential_bitcast_fusion.10 = f32[4,64,64,128]{3,0,2,1:T(4,128)S(1)} fusion(f32[64,4,128]{2,1,0:T(4,128)S(1)} %fusion.156, pred[64,64]{1,0:T(8,128)(4,1)S(1)} %fusion.158), kind=kLoop, calls=%fused_computation.49.clone.1 | loop fusion | flops 4194304 | bytes 8523776 | tf_op jit(solution)/shard_map/while
  16.9 7.3 %fusion.160 = f32[4,64,64]{1,2,0:T(8,128)S(1)} fusion(f32[4,64,64,128]{3,0,2,1:T(4,128)S(1)} %exponential_bitcast_fusion.10, f32[4,128,64]{1,2,0:T(8,128)S(1)} %copy.239, f32[4,128,64]{1,2,0:T(8,128)S(1)} %copy.240), kind=kLoop, calls=%fused_computation.48.clone.1 | loop fusion | flops 6275072 | bytes 8716288 | tf_op jit(solution)/shard_map/while/body/eval_jaxpr/ihd,jhd,ijhd->hij/dot_general | solution.py:84
  25.9 5.9 %exponential_bitcast_fusion.10 = f32[4,64,64,128]{3,0,2,1:T(4,128)S(1)} fusion(f32[64,4,128]{2,1,0:T(4,128)S(1)} %fusion.156, pred[64,64]{1,0:T(8,128)(4,1)S(1)} %fusion.158), kind=kLoop, calls=%fused_computation.49.clone.1 | loop fusion | flops 4194304 | bytes 8523776 | tf_op jit(solution)/shard_map/while
  31.8 7.3 %fusion.160 = f32[4,64,64]{1,2,0:T(8,128)S(1)} fusion(f32[4,64,64,128]{3,0,2,1:T(4,128)S(1)} %exponential_bitcast_fusion.10, f32[4,128,64]{1,2,0:T(8,128)S(1)} %copy.239, f32[4,128,64]{1,2,0:T(8,128)S(1)} %copy.240), kind=kLoop, calls=%fused_computation.48.clone.1 | loop fusion | flops 6275072 | bytes 8716288 | tf_op jit(solution)/shard_map/while/body/eval_jaxpr/ihd,jhd,ijhd->hij/dot_general | solution.py:84
  43.0 29.9 %while.64 = (s32[]{:T(128)}, f32[4,128,128]{2,1,0:T(8,128)S(1)}, f32[4,128]{1,0:T(4,128)S(1)}, f32[2,64,4,128]{3,1,0,2:T(8,128)S(1)}, f32[2,64,4,128]{3,2,1,0:T(...) while((s32[]{:T(128)}, f32[4,128,128]{2,1,0:T(8,128)S(1)}, ...), condition=%wide.region_2.3_spmd.clone, body=%wide.region_0.2_spmd.clone.sunk | while | flops 138826752 | bytes 21328020 | solution.py:98
  43.2 5.9 %exponential_bitcast_fusion.8 = f32[4,64,64,128]{3,0,2,1:T(4,128)S(1)} fusion(f32[64,4,128]{2,1,0:T(4,128)S(1)} %fusion.142, pred[64,64]{1,0:T(8,128)(4,1)S(1)} %fusion.144), kind=kLoop, calls=%fused_computation.10.clone.1 | loop fusion | flops 4194304 | bytes 8523776 | tf_op jit(solution)/shard_map/while
  49.1 7.3 %fusion.146 = f32[4,64,64]{1,2,0:T(8,128)S(1)} fusion(f32[4,64,64,128]{3,0,2,1:T(4,128)S(1)} %exponential_bitcast_fusion.8, f32[4,128,64]{1,2,0:T(8,128)S(1)} %copy.234, f32[4,128,64]{1,2,0:T(8,128)S(1)} %copy.235), kind=kLoop, calls=%fused_computation.9.clone.1 | loop fusion | flops 6275072 | bytes 8716288 | tf_op jit(solution)/shard_map/while/body/eval_jaxpr/ihd,jhd,ijhd->hij/dot_general | solution.py:84
  58.2 5.9 %exponential_bitcast_fusion.8 = f32[4,64,64,128]{3,0,2,1:T(4,128)S(1)} fusion(f32[64,4,128]{2,1,0:T(4,128)S(1)} %fusion.142, pred[64,64]{1,0:T(8,128)(4,1)S(1)} %fusion.144), kind=kLoop, calls=%fused_computation.10.clone.1 | loop fusion | flops 4194304 | bytes 8523776 | tf_op jit(solution)/shard_map/while
  64.1 7.3 %fusion.146 = f32[4,64,64]{1,2,0:T(8,128)S(1)} fusion(f32[4,64,64,128]{3,0,2,1:T(4,128)S(1)} %exponential_bitcast_fusion.8, f32[4,128,64]{1,2,0:T(8,128)S(1)} %copy.234, f32[4,128,64]{1,2,0:T(8,128)S(1)} %copy.235), kind=kLoop, calls=%fused_computation.9.clone.1 | loop fusion | flops 6275072 | bytes 8716288 | tf_op jit(solution)/shard_map/while/body/eval_jaxpr/ihd,jhd,ijhd->hij/dot_general | solution.py:84
  76.6 16.8 %all-gather.5 = bf16[16,4,128]{2,1,0:T(4,128)(2,1)S(1)} all-gather(bf16[1,4,128]{2,1,0:T(4,128)(2,1)S(1)} %convert_bitcast_fusion), channel_id=4, replica_groups=mesh['sp'=16,'tp'=2] {'sp'}, dimensions={0}, use_global_device_ids=true | all-gather | bytes 17408 | tf_op jit(solution)/shard_map/all_gather | solution.py:16
  93.5 18.6 %all-gather.4 = bf16[16,4,128]{2,1,0:T(4,128)(2,1)S(1)} all-gather(bf16[1,4,128]{2,1,0:T(4,128)(2,1)S(1)} %convert_bitcast_fusion.1), channel_id=2, replica_groups=mesh['sp'=16,'tp'=2] {'sp'}, dimensions={0}, use_global_device_ids=true | all-gather | bytes 17408 | tf_op jit(solution)/shard_map/all_gather | solution.py:16
  112.1 18.6 %while.67 = (s32[]{:T(128)}, f32[4,128,128]{2,1,0:T(8,128)S(1)}, s32[]{:T(128)}, bf16[16,4,128]{2,1,0:T(4,128)(2,1)S(1)}, bf16[16,4,128,128]{3,2,1,0:T(8,128)(2,...) while((s32[]{:T(128)}, f32[4,128,128]{2,1,0:T(8,128)S(1)}, s32[]{:T(128)}, ...), condition=%wide.region_9.10_spmd.clone, body=%wide.region_8.9_spmd.clone.sunk | while | flops 328200 | bytes 660647 | solution.py:34
  131.8 18.4 %while.65 = (s32[]{:T(128)}, f32[4,128,128]{2,1,0:T(8,128)S(1)}, s32[]{:T(128)}, bf16[16,4,128]{2,1,0:T(4,128)(2,1)S(1)}, bf16[16,4,128,128]{3,2,1,0:T(8,128)(2,1)}, /*index=5*/s32[]{:T(128)}, s32[]{:T(128)}) while((s32[]{:T(128)}, f32[4,128,128]{2,1,0:T(8,128)S(1)}, s32[]{:T(128)}, bf16[16,4,128]{2,1,0:T(4,128)(2,1)S(1)}, ...), condition=%wide.region_4.5_spmd.clone, body=%wide.region_3.4_spmd.clone.sunk | while | flops 328196 | bytes 660585 | solution.py:34
  131.8 1.1 fusion.148
  151.8 3.5 all-to-all-start
  155.4 4.4 all-to-all-done
  159.8 18.0 %all-gather.13.cloned.1.call-done = bf16[1024,2048]{1,0:T(8,128)(2,1)} async-done(((bf16[1024,128]{1,0:T(8,128)(2,1)}), bf16[1024,2048]{1,0:T(8,128)(2,1)}) %all-gather.13.cloned.1.call-update) | async-done | bytes 4194320 | tf_op jit(solution)/shard_map/all_gather | solution.py:138
  177.8 3.1 multiply_reduce_fusion
  181.1 9.1 %all_gather.48 = bf16[128,2048]{1,0:T(8,128)(2,1)S(1)} all-gather(bf16[64,2048]{1,0:T(8,128)(2,1)S(1)} %multiply_convert_fusion), channel_id=1, replica_groups=mesh['sp'=16,'tp'=2] {'tp'}, dimensions={0}, use_global_device_ids=true | all-gather | bytes 786432 | tf_op jit(solution)/shard_map/all_gather | solution.py:169
  190.3 82.0 %all-gather.17.cloned.1.call-done = bf16[2048,2816]{1,0:T(8,128)(2,1)} async-done(((bf16[128,2816]{1,0:T(8,128)(2,1)}), bf16[2048,2816]{1,0:T(8,128)(2,1)}) %all-gather.17.cloned.1.call-update) | async-done | bytes 11534352 | tf_op jit(solution)/shard_map/all_gather | solution.py:136
  272.3 5.9 %convolution_convert_fusion = bf16[128,2816]{1,0:T(8,128)(2,1)S(1)} fusion(bf16[128,2048]{1,0:T(8,128)(2,1)S(1)} %all_gather.48, bf16[2048,2816]{1,0:T(8,128)(2,1)} %all-gather.17.cloned.1.call-done), kind=kOutput, calls=%fused_computation.86 | convolution fusion | flops 1476755456 | bytes 12779520 | tf_op jit(solution)/shard_map/dot_general | solution.py:171
  278.2 88.4 %all-gather.15.cloned.1.call-done = bf16[2048,2816]{1,0:T(8,128)(2,1)} async-done(((bf16[128,2816]{1,0:T(8,128)(2,1)}), bf16[2048,2816]{1,0:T(8,128)(2,1)}) %all-gather.15.cloned.1.call-update) | async-done | bytes 11534352 | tf_op jit(solution)/shard_map/all_gather | solution.py:135
  366.7 5.9 %convolution_convert_fusion.1 = bf16[128,2816]{1,0:T(8,128)(2,1)S(1)} fusion(bf16[128,2048]{1,0:T(8,128)(2,1)S(1)} %all_gather.48, bf16[2048,2816]{1,0:T(8,128)(2,1)} %all-gather.15.cloned.1.call-done), kind=kOutput, calls=%fused_computation.87 | convolution fusion | flops 1476755456 | bytes 12779520 | tf_op jit(solution)/shard_map/dot_general | solution.py:170
  372.7 2.2 collective-permute-start
  374.8 4.3 collective-permute-start.1
  379.3 1.7 collective-permute-done.1
  381.1 3.2 multiply_add_fusion
  384.3 79.6 %all-gather.19.cloned.1.call-done = bf16[2816,2048]{1,0:T(8,128)(2,1)} async-done(((bf16[2816,128]{1,0:T(8,128)(2,1)}), bf16[2816,2048]{1,0:T(8,128)(2,1)}) %all-gather.19.cloned.1.call-update) | async-done | bytes 11534352 | tf_op jit(solution)/shard_map/all_gather | solution.py:137
  463.9 7.7 %convolution_convert_fusion.2 = bf16[128,2048]{1,0:T(8,128)(2,1)} fusion(bf16[2816,2048]{1,0:T(8,128)(2,1)} %all-gather.19.cloned.1.call-done, f32[128,5632]{1,0:T(8,128)} %multiply_add_fusion), kind=kOutput, calls=%fused_computation.89 | convolution fusion | flops 1478819840 | bytes 14942208 | tf_op jit(solution)/shard_map/dot_general | solution.py:182
  471.7 14.9 %reduce-scatter.2.cloned.1.call-done = bf16[64,2048]{1,0:T(8,128)(2,1)} async-done(((bf16[128,2048]{1,0:T(8,128)(2,1)}), bf16[64,2048]{1,0:T(8,128)(2,1)}) %reduce-scatter.2.cloned.1.call-update) | async-done | bytes 262160 | tf_op jit(solution)/shard_map/reduce_scatter | solution.py:183
  486.5 1.7 add_convert_fusion
  (202 shorter events, 54.4 us)
Async XLA Ops:
  6.5 3.2 copy-start.4
  6.5 3.9 copy-start.1
  6.5 105.5 %all-gather.23.cloned.1.call-start = ((), (), s32[]{:S(2)}) async-start(), calls=%async_computation.8 | async-start | bytes 2228224 | tf_op jit(solution)/shard_map/all_gather | solution.py:16
  10.7 31.6 %copy-start.2 = (bf16[128,512]{1,0:T(8,128)(2,1)S(1)}, bf16[128,512]{1,0:T(8,128)(2,1)}, u32[]{:S(2)}) copy-start(bf16[128,512]{1,0:T(8,128)(2,1)} %param.25) | copy-start | bytes 393220
  41.3 90.4 %all-gather.21.cloned.1.call-start = ((), (), s32[]{:S(2)}) async-start(), calls=%async_computation.7 | async-start | bytes 2228224 | tf_op jit(solution)/shard_map/all_gather | solution.py:16
  72.9 3.5 copy-start.3
  72.9 39.1 %copy-start.5 = (f32[3,2816]{1,0:T(4,128)S(1)}, f32[3,2816]{1,0:T(4,128)}, u32[]{:S(2)}) copy-start(f32[3,2816]{1,0:T(4,128)} %param.37) | copy-start | bytes 101380
  73.6 104.2 %all-gather.13.cloned.1.call-start = ((), (), s32[]{:S(2)}) async-start(), calls=%async_computation.2 | async-start | bytes 4456448 | tf_op jit(solution)/shard_map/all_gather | solution.py:138
  74.4 197.9 %all-gather.17.cloned.1.call-start = ((), (), s32[]{:S(2)}) async-start(), calls=%async_computation.4 | async-start | bytes 12255232 | tf_op jit(solution)/shard_map/all_gather | solution.py:136
  74.9 291.7 %all-gather.15.cloned.1.call-start = ((), (), s32[]{:S(2)}) async-start(), calls=%async_computation.3 | async-start | bytes 12255232 | tf_op jit(solution)/shard_map/all_gather | solution.py:135
  75.5 388.4 %all-gather.19.cloned.1.call-start = ((), (), s32[]{:S(2)}) async-start(), calls=%async_computation.5 | async-start | bytes 12255232 | tf_op jit(solution)/shard_map/all_gather | solution.py:137
  131.3 19.5 %copy-start.8 = (f32[128]{0:T(128)S(1)}, f32[128]{0:T(128)}, u32[]{:S(2)}) copy-start(f32[128]{0:T(128)} %param.32) | copy-start | bytes 1540
  131.7 23.6 %copy-start.6 = (f32[3,2816]{1,0:T(4,128)S(1)}, f32[3,2816]{1,0:T(4,128)}, u32[]{:S(2)}) copy-start(f32[3,2816]{1,0:T(4,128)} %param.38) | copy-start | bytes 101380
  131.8 46.1 %copy-start = (bf16[64,2048]{1,0:T(8,128)(2,1)S(1)}, bf16[64,2048]{1,0:T(8,128)(2,1)}, u32[]{:S(2)}) copy-start(bf16[64,2048]{1,0:T(8,128)(2,1)} %param.24) | copy-start | bytes 786436
  151.8 29.2 %copy-start.7 = (f32[2048]{0:T(1024)S(1)}, f32[2048]{0:T(1024)}, u32[]{:S(2)}) copy-start(f32[2048]{0:T(1024)} %param.34) | copy-start | bytes 24580
  151.8 8.0 %all-to-all-start = ((bf16[2,64,512]{2,1,0:T(8,128)(2,1)}), bf16[2,64,512]{2,1,0:T(8,128)(2,1)S(1)}, u32[]{:S(2)}, u32[]{:S(2)}) async-start(bf16[2,64,512]{2,1,0:T(8,128)(2,1)} %convert_element_type.128), calls=%async_computation | async-start | bytes 262144 | tf_op jit(solution)/shard_map/all_to_all | solution.py:165
  155.3 331.2 %reduce-scatter.2.cloned.1.call-start = ((), (), s32[]{:S(2)}) async-start(), calls=%async_computation.6 | async-start | bytes 786432 | tf_op jit(solution)/shard_map/reduce_scatter | solution.py:183
  372.7 6.7 %collective-permute-start = (bf16[1,5632]{1,0:T(2,128)(2,1)S(1)}, bf16[1,5632]{1,0:T(2,128)(2,1)S(1)}, u32[]{:S(2)}, u32[]{:S(2)}) collective-permute-start(bf16[1,5632]{1,0:T(2,128)(2,1)S(1)} %get-tuple-element.632), channel_id=1, source_target_pairs={{0,2},{2,4},{4,6},{6,8},{8,10},{10,12},{12,14},{14,16},{16,18},{18... | collective-permute-start | bytes 33800 | tf_op jit(solution)/shard_map/ppermute | solution.py:44
  374.8 6.2 %collective-permute-start.1 = (bf16[1,5632]{1,0:T(2,128)(2,1)S(1)}, bf16[1,5632]{1,0:T(2,128)(2,1)S(1)}, u32[]{:S(2)}, u32[]{:S(2)}) collective-permute-start(bf16[1,5632]{1,0:T(2,128)(2,1)S(1)} %get-tuple-element.633), channel_id=1, source_target_pairs={{2,0},{4,2},{6,4},{8,6},{10,8},{12,10},{14,12},{16,14},{18,16},{20... | collective-permute-start | bytes 33800 | tf_op jit(solution)/shard_map/ppermute | solution.py:45
Sparse Core Ops, SparseCore 0:
  41.5 41.1 all-gather.22
  84.9 40.1 all-gather.20
  127.2 50.5 all-gather.12
  180.0 92.2 all-gather.16
  274.4 92.2 all-gather.14
  368.7 95.2 all-gather.18
  471.8 14.6 reduce-scatter.1
where the time goes:
time: 498 us; the launch traced here: 495 us
  waiting for transfers between devices  291 us (58%)
  other arithmetic  98.2 us (20%)
  blocking collectives  44.5 us (9%)
  matrix products  29.6 us (6%)
  between operations  14 us (3%)
  starting transfers between devices  10.4 us (2%)
  local copies, waits for them, and re-layouts  5.26 us (1%)
    all_gather x1, waiting for transfers between devices, on_device(): lax.all_gather(gate_up_matrix, 'sp', axis=0, tiled=True)  88.4 us
    all_gather x1, waiting for transfers between devices, on_device(): lax.all_gather(value_up_matrix, 'sp', axis=0, tiled=True)  82 us
    all_gather x1, waiting for transfers between devices, on_device(): lax.all_gather(down_matrix, 'sp', axis=1, tiled=True)  79.6 us
    all_gather x2, blocking collectives, carried_in(): lax.all_gather(part.astype(kind), axis)  35.4 us
    select_n x32, other arithmetic, hop(): return jax.tree.map(lambda a, b: jnp.where(reached, a, b), new, before)  35.4 us
    dot_general x4, other arithmetic, advance(): jnp.einsum('ihd,jhd,ijhd->hij', query_part, key_part, jnp.exp(gaps), prec...  29.1 us
    while x4, other arithmetic  23.5 us
    all_gather x1, waiting for transfers between devices, on_device(): lax.all_gather(output_matrix, 'sp', axis=1, tiled=True)  18 us
  transfers between devices with their start and end apart: 10, of which 7 were waited for; matrix products, arithmetic and copies ran while one was open for 18% of the time, Pallas kernels for 0%

commit v1 on v0

v1 whole, which is shorter than its diff:
```python
import functools

import jax
import jax.numpy as jnp
from jax import lax
from jax.experimental import pallas as pl
from jax.experimental.pallas import tpu as pltpu
from jax.sharding import PartitionSpec as P

HEAD_WIDTH = 128
EPSILON = 1e-06
PAD = 16
HALO = 8
F32 = jnp.float32
BF16 = jnp.bfloat16
HIGHEST = lax.Precision.HIGHEST
VMEM = 60 * 1024 * 1024


def nt(a, b):
    return lax.dot_general(a, b, (((1,), (1,)), ((), ())), preferred_element_type=F32)


def tn(a, b):
    return lax.dot_general(a, b, (((0,), (0,)), ((), ())), preferred_element_type=F32)


def kernel_call(body, out_shape, *args, flops=10**9):
    n = len(args)
    return pl.pallas_call(
        body,
        out_shape=out_shape,
        in_specs=[pl.BlockSpec(memory_space=pltpu.VMEM)] * n,
        out_specs=jax.tree.map(lambda _: pl.BlockSpec(memory_space=pltpu.VMEM), out_shape),
        compiler_params=pltpu.CompilerParams(vmem_limit_bytes=VMEM),
        cost_estimate=pl.CostEstimate(flops=flops, transcendentals=0, bytes_accessed=10**6),
    )(*args)


def local_body(ff, fb, ql, vw, floor, extra, inside, carry, payload):
    length, width = vw.shape
    heads = width // HEAD_WIDTH
    slices, rows = payload.shape[0], payload.shape[1] - PAD
    per_head = HEAD_WIDTH // rows
    row = lax.broadcasted_iota(jnp.int32, (length, length), 0)
    col = lax.broadcasted_iota(jnp.int32, (length, length), 1)
    seen = (row >= col, row <= col)
    for h in range(heads):
        lanes = slice(h * HEAD_WIDTH, (h + 1) * HEAD_WIDTH)
        q = jax.nn.silu(ql[:, lanes].astype(F32))
        v = vw[:, lanes]
        scores = jnp.zeros((length, length), F32)
        for d, logits in enumerate((ff, fb)):
            z = logits[:, lanes].astype(F32)
            b = floor[d : d + 1, lanes]
            up = jax.nn.sigmoid(z)
            log_forget = jnp.log(b + (1.0 - b) * up) + extra[d, :, h : h + 1]
            key = (1.0 - b) * jax.nn.sigmoid(-z)
            running = jnp.dot(
                seen[d].astype(F32), log_forget, precision=HIGHEST, preferred_element_type=F32
            )
            middle = running[length // 2 : length // 2 + 1]
            total = running[length - 1 : length] if d == 0 else running[0:1]
            rise = jnp.exp(running - middle)
            qd = q * rise
            kd = (key * jnp.exp(middle - running)).astype(BF16)
            scores += jnp.where(seen[d], nt(qd.astype(BF16), kd), 0.0)
            carry[d, :, lanes] = (qd * jnp.exp(middle)).astype(BF16)
            state = (tn(v, kd) * jnp.exp(total - middle)).astype(BF16)
            decay = jnp.exp(total)
            high = decay.astype(BF16)
            low = (decay - high.astype(F32)).astype(BF16)
            tail = jnp.where(
                lax.broadcasted_iota(jnp.int32, (PAD, HEAD_WIDTH), 0) == 0,
                high.astype(F32),
                low.astype(F32),
            ).astype(BF16)
            for i in range(per_head):
                at = (d * heads + h) * per_head + i
                payload[at, 0:rows, :] = state[i * rows : (i + 1) * rows]
                payload[at, rows : rows + PAD, :] = tail
        inside[:, lanes] = jnp.dot(scores.astype(BF16), v, preferred_element_type=F32)


def prefix_body(backward, parts, entering):
    size, rows = entering.shape[0], entering.shape[1]
    flip = backward[0] > 0

    def step(k, state):
        at = jnp.where(flip, size - 1 - k, k)
        entering[at] = state.astype(BF16)
        part = parts[at].astype(F32)
        decay = part[rows : rows + 1] + part[rows + 1 : rows + 2]
        return decay * state + part[0:rows]

    lax.fori_loop(0, size, step, jnp.zeros((rows, HEAD_WIDTH), F32), unroll=True)


def readout_body(inside, carry, entering, gate, scale, gated):
    heads = gated.shape[1] // HEAD_WIDTH
    for h in range(heads):
        lanes = slice(h * HEAD_WIDTH, (h + 1) * HEAD_WIDTH)
        out = inside[:, lanes]
        for d in range(2):
            out = out + nt(carry[d, :, lanes], entering[d, h])
        mean = jnp.mean(out * out, axis=-1, keepdims=True)
        out = out * lax.rsqrt(mean + EPSILON) * scale[...]
        gated[:, lanes] = (out * jax.nn.silu(gate[:, lanes].astype(F32))).astype(BF16)


def convolved(up, taps, own):
    here, before, after = up[0:own], up[own : own + 1], up[own + 1 : own + 2]
    down = jnp.concatenate([before, here[: own - 1]], axis=0)
    ahead = jnp.concatenate([here[1:], after], axis=0)
    return down * taps[0:1] + here * taps[1:2] + ahead * taps[2:3]


def joined(piece):
    return jnp.concatenate([piece[m] for m in range(piece.shape[0])], axis=1)


def up_body(shards, own, n_pieces, x, gate_taps, value_taps, *refs):
    pieces, hidden = refs[:-1], refs[-1]
    width = hidden.shape[2]
    half = x.shape[1] // n_pieces
    ups = []
    for side in range(2):
        total = 0.0
        for p in range(n_pieces):
            total = total + nt(
                x[:, p * half : (p + 1) * half], joined(pieces[side * n_pieces + p])
            )
        ups.append(total.astype(BF16).astype(F32))
    span = own + HALO
    for s in range(shards):
        rows = slice(s * span, (s + 1) * span)
        gate = convolved(ups[0][rows], gate_taps[...], own)
        value = convolved(ups[1][rows], value_taps[...], own)
        hidden[s] = (jax.nn.silu(gate) * value).astype(BF16)


def down_body(hiddens, pieces, *refs):
    hs, ps, out = refs[:hiddens], refs[hiddens : hiddens + pieces * hiddens], refs[-1]
    members = ps[0].shape[0]
    lefts = [h[...] for h in hs]
    for p in range(pieces):
        total = 0.0
        for t in range(hiddens):
            right = joined(ps[t * pieces + p])
            total = total + jnp.dot(lefts[t], right, preferred_element_type=F32)
        out[:, p * members * HEAD_WIDTH : (p + 1) * members * HEAD_WIDTH] = total.astype(BF16)


def on_device(
    residual,
    forget_forward,
    forget_backward,
    value_written,
    query_logits,
    output_gate_logits,
    forget_minimum,
    extra_log_rate,
    head_norm_scale,
    output_matrix,
    prenorm_scale,
    gate_up_matrix,
    value_up_matrix,
    gate_taps,
    value_taps,
    down_matrix,
):
    sp, tp = lax.axis_size("sp"), lax.axis_size("tp")
    s, t = lax.axis_index("sp"), lax.axis_index("tp")
    length, hw = value_written.shape
    heads = hw // HEAD_WIDTH
    own = residual.shape[0]
    model = residual.shape[1]
    lines = sp // 4
    members = lines * 2
    line, side, core = s // 4, (s // 2) % 2, s % 2
    member = line * 2 + core
    columns = [[4 * z + 2 * y + c for z in range(lines) for c in range(2)] for y in range(2)]
    block = model // sp
    width = gate_up_matrix.shape[1] // members

    def swap_side(a):
        return lax.ppermute(a, "sp", [(i, i ^ 2) for i in range(sp)])

    def swap_core(a):
        return lax.ppermute(a, "sp", [(i, i ^ 1) for i in range(sp)])

    def from_line(a, k):
        return lax.ppermute(a, "sp", [(i, (i + 4 * k) % sp) for i in range(sp)])

    def from_rank(a, k):
        return lax.ppermute(a, "tp", [(i, (i + k) % tp) for i in range(tp)])

    rows = 2 * heads * HEAD_WIDTH // sp
    inside, carry, payload = kernel_call(
        local_body,
        (
            jax.ShapeDtypeStruct((length, hw), F32),
            jax.ShapeDtypeStruct((2, length, hw), BF16),
            jax.ShapeDtypeStruct((sp, rows + PAD, HEAD_WIDTH), BF16),
        ),
        forget_forward,
        forget_backward,
        query_logits,
        value_written,
        forget_minimum,
        extra_log_rate,
    )
    parts = lax.all_to_all(payload, "sp", 0, 0, tiled=True)
    backward = (s * rows >= heads * HEAD_WIDTH).astype(jnp.int32).reshape(1)
    prefix = pl.pallas_call(
        prefix_body,
        out_shape=jax.ShapeDtypeStruct((sp, rows, HEAD_WIDTH), BF16),
        in_specs=[
            pl.BlockSpec(memory_space=pltpu.SMEM),
            pl.BlockSpec(memory_space=pltpu.VMEM),
        ],
        out_specs=pl.BlockSpec(memory_space=pltpu.VMEM),
    )(backward, parts)
    entering = lax.all_to_all(prefix, "sp", 0, 0, tiled=True)
    entering = entering.reshape(2, heads, HEAD_WIDTH, HEAD_WIDTH)
    gated = kernel_call(
        readout_body,
        jax.ShapeDtypeStruct((length, hw), BF16),
        inside,
        carry,
        entering,
        output_gate_logits,
        head_norm_scale.reshape(1, HEAD_WIDTH),
    )

    out_rows = lax.dynamic_slice_in_dim(output_matrix, t * hw, hw, 0)
    out_own = lax.all_gather(
        out_rows, "sp", axis_index_groups=columns, axis=0
    )
    out_both = jnp.stack([out_own, swap_side(out_own)])

    def by_side(a, axis):
        shape = a.shape[:axis] + (lines, 2, 2, block) + a.shape[axis + 1 :]
        a = jnp.moveaxis(a.reshape(shape), axis + 1, axis)
        first = lax.dynamic_index_in_dim(a, side, axis, keepdims=True)
        second = lax.dynamic_index_in_dim(a, 1 - side, axis, keepdims=True)
        return jnp.concatenate([first, second], axis).reshape(
            a.shape[:axis] + (model,) + a.shape[axis + 4 :]
        )

    part = jnp.einsum("tk,ymkn->tymn", gated, out_both, preferred_element_type=F32)
    part = part.reshape(length, model)
    mixed = lax.dynamic_slice_in_dim(part, t * own, own, 0)
    for k in range(1, tp):
        to = (t + k) % tp
        sent = lax.dynamic_slice_in_dim(part, to * own, own, 0).astype(BF16)
        mixed = mixed + from_rank(sent, k).astype(F32)
    after = by_side(residual, 1).astype(F32) + mixed
    scale = lax.rsqrt(jnp.mean(after * after, axis=-1, keepdims=True) + EPSILON)
    normed = (after * scale * by_side(prenorm_scale, 0)).astype(BF16)

    count = sp * tp
    ahead = [(i, i + 1) for i in range(count - 1)]
    behind = [(i + 1, i) for i in range(count - 1)]
    def natural(a):
        a = a.reshape(a.shape[0], 2, lines, 2, block)
        low = lax.dynamic_index_in_dim(a, side, 1, keepdims=True)
        high = lax.dynamic_index_in_dim(a, 1 - side, 1, keepdims=True)
        return jnp.moveaxis(jnp.concatenate([low, high], 1), 1, 2).reshape(a.shape[0], model)

    edges = natural(jnp.concatenate([normed[:1], normed[own - 1 :]], 0))
    before = lax.ppermute(edges[1:2], ("sp", "tp"), ahead)
    following = lax.ppermute(edges[0:1], ("sp", "tp"), behind)
    halo = by_side(jnp.concatenate([before, following], 0), 1)
    halo = jnp.pad(halo, ((0, HALO - 2), (0, 0)))
    shard = jnp.concatenate([normed, halo], 0)
    shards = [shard] + [from_line(shard, k) for k in range(1, lines)]
    tokens = jnp.concatenate(shards, 0)
    tokens = jnp.concatenate([tokens, swap_core(tokens)], 0)

    def spread(piece):
        got = lax.all_to_all(piece, "sp", 0, 0, axis_index_groups=columns, tiled=True)
        pieces = [(got, swap_side(got))]
        cut = members // 2
        for k in range(1, tp):
            rank = from_rank(got, k)
            low = swap_side(rank[:cut])
            high = from_rank(pieces[0][1][cut:], k)
            pieces.append((rank, jnp.concatenate([low, high], 0)))
        return pieces

    gates = spread(gate_up_matrix.T.reshape(members, width, block))
    values = spread(value_up_matrix.T.reshape(members, width, block))
    downs = spread(down_matrix.reshape(members, width, block))
    taps = jnp.concatenate([gate_taps, value_taps], 0)
    taps = lax.dynamic_slice_in_dim(taps, member * width, width, 1)
    taps = [taps] + [from_rank(taps, k) for k in range(1, tp)]

    plain = block == HEAD_WIDTH
    hiddens = []
    for k in range(tp):
        if plain:
            hidden = kernel_call(
                functools.partial(up_body, members, own, 2),
                jax.ShapeDtypeStruct((members, own, width), BF16),
                tokens,
                taps[k][:3],
                taps[k][3:],
                *gates[k],
                *values[k],
            ).reshape(members * own, width)
        else:
            x = tokens.reshape(-1, 2, members, block)
            up = [
                jnp.einsum("nymd,ymhd->nh", x, jnp.stack(w[k]), preferred_element_type=F32)
                .astype(BF16)
                .reshape(members, own + HALO, width)
                for w in (gates, values)
            ]
            conv = jax.vmap(convolved, (0, None, None))
            hidden = (jax.nn.silu(conv(up[0], taps[k][:3], own)) * conv(up[1], taps[k][3:], own))
            hidden = hidden.astype(BF16).reshape(members * own, width)
        hiddens.append(hidden)
    if plain:
        terms = kernel_call(
            functools.partial(down_body, tp, 2),
            jax.ShapeDtypeStruct((members * own, model), BF16),
            *hiddens,
            *[p for k in range(tp) for p in downs[k]],
        )
    else:
        terms = sum(
            jnp.einsum("nh,ymhd->nymd", hiddens[k], jnp.stack(downs[k]), preferred_element_type=F32)
            for k in range(tp)
        )
        terms = terms.astype(BF16).reshape(members * own, model)

    half = lines * own
    terms = terms[:half].astype(F32) + swap_core(terms[half:]).astype(F32)
    total = after + terms[:own]
    for k in range(1, lines):
        sent = terms[k * own : (k + 1) * own].astype(BF16)
        total = total + from_line(sent, lines - k).astype(F32)
    return natural(total).astype(BF16)


def solution(mesh):
    return jax.shard_map(
        on_device,
        mesh=mesh,
        in_specs=(
            P(("sp", "tp"), None),
            P("sp", "tp"),
            P("sp", "tp"),
            P("sp", "tp"),
            P("sp", "tp"),
            P("sp", "tp"),
            P(None, "tp"),
            P(None, "sp", "tp"),
            P(),
            P(None, "sp"),
            P(),
            P("sp", "tp"),
            P("sp", "tp"),
            P(None, "tp"),
            P(None, "tp"),
            P("tp", "sp"),
        ),
        out_specs=P(("sp", "tp"), None),
        check_vma=False,
    )
```

time: 498 us -> 259 us (0.52)
  waiting for transfers between devices: 291 us -> 118 us
  other arithmetic: 98.2 us -> 6.88 us
  starting transfers between devices: 10.4 us -> 64.5 us
  blocking collectives: 44.5 us -> 0 us
  matrix products: 29.6 us -> 2.24 us
  Pallas kernels: 0 us -> 26 us
  local copies, waits for them, and re-layouts: 5.26 us -> 26.3 us
    all_gather x6 -> x1, waiting for transfers between devices: 268 us -> 0.01 us  [on_device(): out_own = lax.all_gather(out_rows, 'sp', axis_index_groups=columns, axis=0)]
    ppermute x2 -> x25, waiting for transfers between devices: 1.71 us -> 94.8 us  [the longest x6 54.6 us: from_line(): return lax.ppermute(a, 'sp', [(i, (i + 4 * k) % sp) for i in range(sp)])]
    all_gather x3 -> x0, blocking collectives: 44.5 us -> none  [the longest x2 35.4 us: carried_in(): lax.all_gather(part.astype(kind), axis)]
    select_n x32 -> x0, other arithmetic: 35.4 us -> none  [hop(): return jax.tree.map(lambda a, b: jnp.where(reached, a, b), new, before)]
    dot_general x4 -> x0, other arithmetic: 29.1 us -> none  [advance(): jnp.einsum('ihd,jhd,ijhd->hij', query_part, key_part, jnp.exp(gaps), prec...]
    all_to_all x1 -> x5, starting transfers between devices: 3.51 us -> 31.9 us  [the longest x3 18.8 us: spread(): lax.all_to_all(piece, 'sp', 0, 0, axis_index_groups=columns, tiled=True)]
    dot_general x18 -> x1, matrix products: 29.6 us -> 2.24 us  [on_device(): jnp.einsum('tk,ymkn->tymn', gated, out_both, preferred_element_type=F32)]
    ppermute x2 -> x25, starting transfers between devices: 6.46 us -> 32.6 us  [the longest x6 12.7 us: from_line(): return lax.ppermute(a, 'sp', [(i, (i + 4 * k) % sp) for i in range(sp)])]
  transfers between devices with their start and end apart: 10 -> 31, of which waited for: 7 -> 15; matrix products, arithmetic and copies ran while one was open for 18% -> 11% of each run, Pallas kernels for 0% -> 3%
where the time goes in v1:
time: 259 us; the launch traced here: 258 us
  waiting for transfers between devices  118 us (46%)
  starting transfers between devices  64.5 us (25%)
  local copies, waits for them, and re-layouts  26.3 us (10%)
  Pallas kernels  26 us (10%)
  between operations  13.8 us (5%)
  other arithmetic  6.88 us (3%)
    ppermute x6, waiting for transfers between devices, from_line(): return lax.ppermute(a, 'sp', [(i, (i + 4 * k) % sp) for i in range(sp)])  54.6 us
    pallas_call x5, Pallas kernels, kernel_call(): pl.pallas_call(body, out_shape=out_shape, in_specs=[pl.BlockSpec(memory_s...  24.3 us
    ppermute x8, waiting for transfers between devices, from_rank(): return lax.ppermute(a, 'tp', [(i, (i + k) % tp) for i in range(tp)])  20.5 us
    all_to_all x3, starting transfers between devices, spread(): lax.all_to_all(piece, 'sp', 0, 0, axis_index_groups=columns, tiled=True)  18.8 us
    ppermute x7, waiting for transfers between devices, swap_side(): return lax.ppermute(a, 'sp', [(i, i ^ 2) for i in range(sp)])  17 us
    all_to_all x1, waiting for transfers between devices, on_device(): parts = lax.all_to_all(payload, 'sp', 0, 0, tiled=True)  13.2 us
    ppermute x6, starting transfers between devices, from_line(): return lax.ppermute(a, 'sp', [(i, (i + 4 * k) % sp) for i in range(sp)])  12.7 us
    unnamed x38, local copies, waits for them, and re-layouts  9 us
  transfers between devices with their start and end apart: 31, of which 15 were waited for; matrix products, arithmetic and copies ran while one was open for 11% of the time, Pallas kernels for 3%

profile of v1, /device:TPU:24, one launch (start us, length us, event | category | flops | bytes accessed | tf_op | source)
XLA Modules:
  0.0 258.0 jit_solution(3881092723572356243)
XLA Ops:
  9.7 4.2 %shard_map.154 = (f32[128,512]{1,0:T(8,128)}, bf16[2,128,512]{2,1,0:T(8,128)(2,1)}, bf16[16,80,128]{2,1,0:T(8,128)(2,1)}) custom-call(bf16[128,512]{1,0:T(8,128)(2,1)} %ff.1, bf16[128,512]{1,0:T(8,128)(2,1)} %fb.1, bf16[128,512]{1,0:T(8,128)(2,1)} %ql.1, bf16[128,512]{1,0:T(8,128)(2,1)} %vw.1, f32[2,512]{1,0:T(2,128)} %floor.1, f32[2,128,4]{2,1,0:T(8,128)} %copy.22.extra), custom_call_target="tpu_custom_call" | custom-call | flops 1000000000 | bytes 1000000 | tf_op jit(solution)/shard_map/pallas_call | solution.py:30
  13.8 6.2 %all-to-all-start = ((bf16[16,80,128]{2,1,0:T(8,128)(2,1)}), bf16[16,80,128]{2,1,0:T(8,128)(2,1)S(1)}, u32[]{:S(2)}, u32[]{:S(2)}) async-start(bf16[16,80,128]{2,1,0:T(8,128)(2,1)} %get-tuple-element.10), calls=%async_computation | async-start | bytes 655360 | tf_op jit(solution)/shard_map/all_to_all | solution.py:213
  20.0 13.2 %all-to-all-done.parts = bf16[16,80,128]{2,1,0:T(8,128)(2,1)S(1)} async-done(((bf16[16,80,128]{2,1,0:T(8,128)(2,1)}), bf16[16,80,128]{2,1,0:T(8,128)(2,1)S(1)}, u32[]{:S(2)}, u32[]{:S(2)}) %all-to-all-start) | async-done | bytes 327712 | tf_op jit(solution)/shard_map/all_to_all | solution.py:213
  33.9 1.7 shard_map.155
  35.7 6.9 %all-to-all-start.1 = ((bf16[16,64,128]{2,1,0:T(8,128)(2,1)}), bf16[16,64,128]{2,1,0:T(8,128)(2,1)S(1)}, u32[]{:S(2)}, u32[]{:S(2)}) async-start(bf16[16,64,128]{2,1,0:T(8,128)(2,1)} %shard_map.155), calls=%async_computation.1 | async-start | bytes 524288 | tf_op jit(solution)/shard_map/all_to_all | solution.py:224
  46.8 3.0 %all-to-all-done.1 = bf16[16,64,128]{2,1,0:T(8,128)(2,1)S(1)} async-done(((bf16[16,64,128]{2,1,0:T(8,128)(2,1)}), bf16[16,64,128]{2,1,0:T(8,128)(2,1)S(1)}, u32[]{:S(2)}, u32[]{:S(2)}) %all-to-all-start.1) | async-done | bytes 262176 | tf_op jit(solution)/shard_map/all_to_all | solution.py:224
  49.8 7.0 %all-to-all-start.2 = ((bf16[8,352,128]{2,1,0:T(8,128)(2,1)}), bf16[8,352,128]{2,1,0:T(8,128)(2,1)}, u32[]{:S(2)}, u32[]{:S(2)}) async-start(bf16[8,352,128]{2,1,0:T(8,128)(2,1)} %bitcast.19), calls=%async_computation.2 | async-start | bytes 1441792 | tf_op jit(solution)/shard_map/all_to_all | solution.py:282
  57.6 2.3 shard_map.156
  61.2 9.5 %collective-permute-done = bf16[8,512,128]{1,2,0:T(8,128)(2,1)} collective-permute-done((bf16[8,512,128]{1,2,0:T(8,128)(2,1)S(1)}, bf16[8,512,128]{1,2,0:T(8,128)(2,1)}, u32[]{:S(2)}, u32[]{:S(2)}) %collective-permute-start) | collective-permute-done | bytes 1048608 | tf_op jit(solution)/shard_map/ppermute | solution.py:187
  70.7 2.2 fusion
  77.1 5.1 %all-to-all-start.3 = ((bf16[8,352,128]{2,1,0:T(8,128)(2,1)}), bf16[8,352,128]{2,1,0:T(8,128)(2,1)}, u32[]{:S(2)}, u32[]{:S(2)}) async-start(bf16[8,352,128]{2,1,0:T(8,128)(2,1)} %bitcast.21), calls=%async_computation.3 | async-start | bytes 1441792 | tf_op jit(solution)/shard_map/all_to_all | solution.py:282
  86.2 2.2 collective-permute-start.3
  88.4 3.7 %collective-permute-start.2 = (bf16[1,2048]{1,0:T(2,128)(2,1)S(1)}, bf16[1,2048]{1,0:T(2,128)(2,1)S(1)}, u32[]{:S(2)}, u32[]{:S(2)}) collective-permute-start(bf16[1,2048]{1,0:T(2,128)(2,1)S(1)} %slice.72), channel_id=1, source_target_pairs={{0,1},{1,2},{2,3},{3,4},{4,5},{5,6},{6,7},{7,8},{8,9},{9,10},{10,1... | collective-permute-start | bytes 12296 | tf_op jit(solution)/shard_map/ppermute | solution.py:272
  92.1 7.2 %all-to-all-done.3.refs_2_ = bf16[8,352,128]{2,1,0:T(8,128)(2,1)} async-done(((bf16[8,352,128]{2,1,0:T(8,128)(2,1)}), bf16[8,352,128]{2,1,0:T(8,128)(2,1)}, u32[]{:S(2)}, u32[]{:S(2)}) %all-to-all-start.3) | async-done | bytes 720928 | tf_op jit(solution)/shard_map/all_to_all | solution.py:282
  99.3 6.7 %all-to-all-start.4 = ((bf16[8,352,128]{2,1,0:T(8,128)(2,1)}), bf16[8,352,128]{2,1,0:T(8,128)(2,1)}, u32[]{:S(2)}, u32[]{:S(2)}) async-start(bf16[8,352,128]{2,1,0:T(8,128)(2,1)} %bitcast.49), calls=%async_computation.4 | async-start | bytes 1441792 | tf_op jit(solution)/shard_map/all_to_all | solution.py:282
  107.6 1.9 collective-permute-start.5
  110.7 3.1 %collective-permute-done.10 = f32[6,352]{1,0:T(8,128)S(1)} collective-permute-done((f32[6,352]{1,0:T(8,128)S(1)}, f32[6,352]{1,0:T(8,128)S(1)}, u32[]{:S(2)}, u32[]{:S(2)}) %collective-permute-start.10) | collective-permute-done | bytes 8480 | tf_op jit(solution)/shard_map/ppermute | solution.py:196
  115.6 10.0 %collective-permute-done.4 = bf16[72,2048]{1,0:T(8,128)(2,1)S(1)} collective-permute-done((bf16[72,2048]{1,0:T(8,128)(2,1)}, bf16[72,2048]{1,0:T(8,128)(2,1)S(1)}, u32[]{:S(2)}, u32[]{:S(2)}) %collective-permute-start.4) | collective-permute-done | bytes 294944 | tf_op jit(solution)/shard_map/ppermute | solution.py:193
  127.0 21.4 %collective-permute-done.5 = bf16[72,2048]{1,0:T(8,128)(2,1)} collective-permute-done((bf16[72,2048]{1,0:T(8,128)(2,1)}, bf16[72,2048]{1,0:T(8,128)(2,1)}, u32[]{:S(2)}, u32[]{:S(2)}) %collective-permute-start.5) | collective-permute-done | bytes 294944 | tf_op jit(solution)/shard_map/ppermute | solution.py:193
  150.2 1.7 constant_dynamic-update-slice_fusion.1
  151.9 1.8 constant_dynamic-update-slice_fusion
  160.1 7.5 %collective-permute-done.17.refs_3_ = bf16[8,352,128]{2,1,0:T(8,128)(2,1)S(1)} collective-permute-done((bf16[8,352,128]{2,1,0:T(8,128)(2,1)}, bf16[8,352,128]{2,1,0:T(8,128)(2,1)S(1)}, u32[]{:S(2)}, u32[]{:S(2)}) %collective-permute-start.17) | collective-permute-done | bytes 720928 | tf_op jit(solution)/shard_map/ppermute | solution.py:187
  170.3 6.2 %collective-permute-done.13 = bf16[4,352,128]{2,1,0:T(8,128)(2,1)S(1)} collective-permute-done((bf16[4,352,128]{2,1,0:T(8,128)(2,1)S(1)}, bf16[4,352,128]{2,1,0:T(8,128)(2,1)S(1)}, u32[]{:S(2)}, u32[]{:S(2)}) %collective-permute-start.13) | collective-permute-done | bytes 360480 | tf_op jit(solution)/shard_map/ppermute | solution.py:196
  179.5 4.8 %collective-permute-done.16 = bf16[4,352,128]{2,1,0:T(8,128)(2,1)S(1)} collective-permute-done((bf16[4,352,128]{2,1,0:T(8,128)(2,1)S(1)}, bf16[4,352,128]{2,1,0:T(8,128)(2,1)S(1)}, u32[]{:S(2)}, u32[]{:S(2)}) %collective-permute-start.16) | collective-permute-done | bytes 360480 | tf_op jit(solution)/shard_map/ppermute | solution.py:196
  185.2 5.6 %collective-permute-done.20 = bf16[4,352,128]{2,1,0:T(8,128)(2,1)S(1)} collective-permute-done((bf16[4,352,128]{2,1,0:T(8,128)(2,1)S(1)}, bf16[4,352,128]{2,1,0:T(8,128)(2,1)S(1)}, u32[]{:S(2)}, u32[]{:S(2)}) %collective-permute-start.20) | collective-permute-done | bytes 360480 | tf_op jit(solution)/shard_map/ppermute | solution.py:196
  193.2 6.1 %shard_map.157 = bf16[8,64,352]{2,1,0:T(8,128)(2,1)} custom-call(bf16[576,2048]{1,0:T(8,128)(2,1)} %copy-done.1, f32[3,352]{1,0:T(4,128)} %get-tuple-element.35.gate_taps, f32[3,352]{1,0:T(4,128)} %get-tuple-element.34.value_taps, bf16[8,352,128]{2,1,0:T(8,128)(2,1)} %all-to-all-done.2.refs_0_, bf16[8,352,128]{2,1,0:T(8,128)(2,1)} %collective-permute-done.8.refs_1_, ...), custom_call_target="tpu_custom_call" | custom-call | flops 1000000000 | bytes 1000000 | tf_op jit(solution)/shard_map/pallas_call | solution.py:30
  199.3 6.1 %shard_map.158 = bf16[8,64,352]{2,1,0:T(8,128)(2,1)} custom-call(bf16[576,2048]{1,0:T(8,128)(2,1)} %copy-done.1, f32[3,352]{1,0:T(4,128)} %get-tuple-element.33.gate_taps, f32[3,352]{1,0:T(4,128)} %get-tuple-element.32.value_taps, bf16[8,352,128]{2,1,0:T(8,128)(2,1)} %collective-permute-done.11.refs_0_, bf16[8,352,128]{2,1,0:T(8,128)(2,1)} %pad_maximum_fusion.refs_1_, ...), custom_call_target="tpu_custom_call" | custom-call | flops 1000000000 | bytes 1000000 | tf_op jit(solution)/shard_map/pallas_call | solution.py:30
  205.4 5.7 %shard_map.159 = bf16[512,2048]{1,0:T(8,128)(2,1)} custom-call(bf16[512,352]{1,0:T(8,128)(2,1)} %bitcast.45, bf16[512,352]{1,0:T(8,128)(2,1)} %bitcast.46, bf16[8,352,128]{2,1,0:T(8,128)(2,1)} %all-to-all-done.4.refs_2_, bf16[8,352,128]{2,1,0:T(8,128)(2,1)} %copy-done.4, bf16[8,352,128]{2,1,0:T(8,128)(2,1)} %copy-done.5, ...), custom_call_target="tpu_custom_call" | custom-call | flops 1000000000 | bytes 1000000 | tf_op jit(solution)/shard_map/pallas_call | solution.py:30
  212.6 2.6 %collective-permute-done.21 = bf16[256,2048]{1,0:T(8,128)(2,1)S(1)} collective-permute-done((bf16[256,2048]{1,0:T(8,128)(2,1)S(1)}, bf16[256,2048]{1,0:T(8,128)(2,1)S(1)}, u32[]{:S(2)}, u32[]{:S(2)}) %collective-permute-start.21) | collective-permute-done | bytes 1048608 | tf_op jit(solution)/shard_map/ppermute | solution.py:190
  215.9 10.1 %collective-permute-start.23 = (bf16[64,2048]{1,0:T(8,128)(2,1)S(1)}, bf16[64,2048]{1,0:T(8,128)(2,1)S(1)}, u32[]{:S(2)}, u32[]{:S(2)}) collective-permute-start(bf16[64,2048]{1,0:T(8,128)(2,1)S(1)} %get-tuple-element.19), channel_id=1, source_target_pairs={{0,16},{2,18},{4,20},{6,22},{8,24},{10,26},{12,28},{14,30},{16,0},... | collective-permute-start | bytes 786440 | tf_op jit(solution)/shard_map/ppermute | solution.py:193
  226.0 5.1 %collective-permute-done.24 = bf16[64,2048]{1,0:T(8,128)(2,1)S(1)} collective-permute-done((bf16[64,2048]{1,0:T(8,128)(2,1)S(1)}, bf16[64,2048]{1,0:T(8,128)(2,1)S(1)}, u32[]{:S(2)}, u32[]{:S(2)}) %collective-permute-start.24) | collective-permute-done | bytes 262176 | tf_op jit(solution)/shard_map/ppermute | solution.py:193
  231.1 18.0 %collective-permute-done.23 = bf16[64,2048]{1,0:T(8,128)(2,1)S(1)} collective-permute-done((bf16[64,2048]{1,0:T(8,128)(2,1)S(1)}, bf16[64,2048]{1,0:T(8,128)(2,1)S(1)}, u32[]{:S(2)}, u32[]{:S(2)}) %collective-permute-start.23) | collective-permute-done | bytes 262176 | tf_op jit(solution)/shard_map/ppermute | solution.py:193
  (128 shorter events, 45.1 us)
Async XLA Ops:
  6.5 36.1 %all-gather.3.cloned.1.call-start = ((), (), s32[]{:S(2)}) async-start(), calls=%async_computation.5 | async-start | bytes 1179648 | tf_op jit(solution)/shard_map/all_gather | solution.py:237
  13.8 31.9 %copy-start.7 = (bf16[128,2816]{1,0:T(8,128)(2,1)S(1)}, bf16[128,2816]{1,0:T(8,128)(2,1)}, u32[]{:S(2)}) copy-start(bf16[128,2816]{1,0:T(8,128)(2,1)} %param.27) | copy-start | bytes 2162692
  13.8 19.4 %all-to-all-start = ((bf16[16,80,128]{2,1,0:T(8,128)(2,1)}), bf16[16,80,128]{2,1,0:T(8,128)(2,1)S(1)}, u32[]{:S(2)}, u32[]{:S(2)}) async-start(bf16[16,80,128]{2,1,0:T(8,128)(2,1)} %get-tuple-element.10), calls=%async_computation | async-start | bytes 655360 | tf_op jit(solution)/shard_map/all_to_all | solution.py:213
  35.7 14.2 %all-to-all-start.1 = ((bf16[16,64,128]{2,1,0:T(8,128)(2,1)}), bf16[16,64,128]{2,1,0:T(8,128)(2,1)S(1)}, u32[]{:S(2)}, u32[]{:S(2)}) async-start(bf16[16,64,128]{2,1,0:T(8,128)(2,1)} %shard_map.155), calls=%async_computation.1 | async-start | bytes 524288 | tf_op jit(solution)/shard_map/all_to_all | solution.py:224
  44.2 26.5 %collective-permute-start = (bf16[8,512,128]{1,2,0:T(8,128)(2,1)S(1)}, bf16[8,512,128]{1,2,0:T(8,128)(2,1)}, u32[]{:S(2)}, u32[]{:S(2)}) collective-permute-start(bf16[8,512,128]{1,2,0:T(8,128)(2,1)S(1)} %copy.23), channel_id=1, source_target_pairs={{0,4},{2,6},{4,0},{6,2},{8,12},{10,14},{12,8},{14,10},{16,20},{18,... | collective-permute-start | bytes 3145736 | tf_op jit(solution)/shard_map/ppermute | solution.py:187
  49.8 27.3 %all-to-all-start.2 = ((bf16[8,352,128]{2,1,0:T(8,128)(2,1)}), bf16[8,352,128]{2,1,0:T(8,128)(2,1)}, u32[]{:S(2)}, u32[]{:S(2)}) async-start(bf16[8,352,128]{2,1,0:T(8,128)(2,1)} %bitcast.19), calls=%async_computation.2 | async-start | bytes 1441792 | tf_op jit(solution)/shard_map/all_to_all | solution.py:282
  74.0 10.0 %collective-permute-start.1 = (bf16[64,2048]{1,0:T(8,128)(2,1)}, bf16[64,2048]{1,0:T(8,128)(2,1)}, u32[]{:S(2)}, u32[]{:S(2)}) collective-permute-start(bf16[64,2048]{1,0:T(8,128)(2,1)} %copy.34), channel_id=1, source_target_pairs={{0,1},{1,0},{2,3},{3,2},{4,5},{5,4},{6,7},{7,6},{8,9},{9,8},{10,11... | collective-permute-start | bytes 786440 | tf_op jit(solution)/shard_map/ppermute | solution.py:196
  77.1 22.2 %all-to-all-start.3 = ((bf16[8,352,128]{2,1,0:T(8,128)(2,1)}), bf16[8,352,128]{2,1,0:T(8,128)(2,1)}, u32[]{:S(2)}, u32[]{:S(2)}) async-start(bf16[8,352,128]{2,1,0:T(8,128)(2,1)} %bitcast.21), calls=%async_computation.3 | async-start | bytes 1441792 | tf_op jit(solution)/shard_map/all_to_all | solution.py:282
  82.2 32.2 %collective-permute-start.8 = (bf16[8,352,128]{2,1,0:T(8,128)(2,1)}, bf16[8,352,128]{2,1,0:T(8,128)(2,1)}, u32[]{:S(2)}, u32[]{:S(2)}) collective-permute-start(bf16[8,352,128]{2,1,0:T(8,128)(2,1)} %all-to-all-done.2.refs_0_), channel_id=1, source_target_pairs={{0,4},{2,6},{4,0},{6,2},{8,12},{10,14},{12,8},{14,10},{16,20},{18,... | collective-permute-start | bytes 2162696 | tf_op jit(solution)/shard_map/ppermute | solution.py:187
  86.2 19.8 %collective-permute-start.3 = (bf16[1,2048]{1,0:T(2,128)(2,1)S(1)}, bf16[1,2048]{1,0:T(2,128)(2,1)S(1)}, u32[]{:S(2)}, u32[]{:S(2)}) collective-permute-start(bf16[1,2048]{1,0:T(2,128)(2,1)S(1)} %slice.74), channel_id=1, source_target_pairs={{1,0},{2,1},{3,2},{4,3},{5,4},{6,5},{7,6},{8,7},{9,8},{10,9},{11,1... | collective-permute-start | bytes 12296 | tf_op jit(solution)/shard_map/ppermute | solution.py:273
  88.4 17.6 %collective-permute-start.2 = (bf16[1,2048]{1,0:T(2,128)(2,1)S(1)}, bf16[1,2048]{1,0:T(2,128)(2,1)S(1)}, u32[]{:S(2)}, u32[]{:S(2)}) collective-permute-start(bf16[1,2048]{1,0:T(2,128)(2,1)S(1)} %slice.72), channel_id=1, source_target_pairs={{0,1},{1,2},{2,3},{3,4},{4,5},{5,6},{6,7},{7,8},{8,9},{9,10},{10,1... | collective-permute-start | bytes 12296 | tf_op jit(solution)/shard_map/ppermute | solution.py:272
  99.3 27.6 %all-to-all-start.4 = ((bf16[8,352,128]{2,1,0:T(8,128)(2,1)}), bf16[8,352,128]{2,1,0:T(8,128)(2,1)}, u32[]{:S(2)}, u32[]{:S(2)}) async-start(bf16[8,352,128]{2,1,0:T(8,128)(2,1)} %bitcast.49), calls=%async_computation.4 | async-start | bytes 1441792 | tf_op jit(solution)/shard_map/all_to_all | solution.py:282
  107.5 18.1 %collective-permute-start.4 = (bf16[72,2048]{1,0:T(8,128)(2,1)}, bf16[72,2048]{1,0:T(8,128)(2,1)S(1)}, u32[]{:S(2)}, u32[]{:S(2)}) collective-permute-start(bf16[72,2048]{1,0:T(8,128)(2,1)} %pad_maximum_fusion.3), channel_id=1, source_target_pairs={{0,8},{2,10},{4,12},{6,14},{8,16},{10,18},{12,20},{14,22},{16,24},... | collective-permute-start | bytes 884744 | tf_op jit(solution)/shard_map/ppermute | solution.py:193
  107.6 40.8 %collective-permute-start.5 = (bf16[72,2048]{1,0:T(8,128)(2,1)}, bf16[72,2048]{1,0:T(8,128)(2,1)}, u32[]{:S(2)}, u32[]{:S(2)}) collective-permute-start(bf16[72,2048]{1,0:T(8,128)(2,1)} %pad_maximum_fusion.3), channel_id=1, source_target_pairs={{0,16},{2,18},{4,20},{6,22},{8,24},{10,26},{12,28},{14,30},{16,0},... | collective-permute-start | bytes 884744 | tf_op jit(solution)/shard_map/ppermute | solution.py:193
  109.5 40.1 %collective-permute-start.6 = (bf16[72,2048]{1,0:T(8,128)(2,1)}, bf16[72,2048]{1,0:T(8,128)(2,1)}, u32[]{:S(2)}, u32[]{:S(2)}) collective-permute-start(bf16[72,2048]{1,0:T(8,128)(2,1)} %pad_maximum_fusion.3), channel_id=1, source_target_pairs={{0,24},{2,26},{4,28},{6,30},{8,0},{10,2},{12,4},{14,6},{16,8},{18,... | collective-permute-start | bytes 884744 | tf_op jit(solution)/shard_map/ppermute | solution.py:193
  110.1 3.7 %collective-permute-start.10 = (f32[6,352]{1,0:T(8,128)S(1)}, f32[6,352]{1,0:T(8,128)S(1)}, u32[]{:S(2)}, u32[]{:S(2)}) collective-permute-start(f32[6,352]{1,0:T(8,128)S(1)} %fusion.8), channel_id=1, source_target_pairs={{0,1},{1,0},{2,3},{3,2},{4,5},{5,4},{6,7},{7,6},{8,9},{9,8},{10,11... | collective-permute-start | bytes 25352 | tf_op jit(solution)/shard_map/ppermute | solution.py:196
  113.8 39.8 %collective-permute-start.11 = (bf16[8,352,128]{2,1,0:T(8,128)(2,1)}, bf16[8,352,128]{2,1,0:T(8,128)(2,1)}, u32[]{:S(2)}, u32[]{:S(2)}) collective-permute-start(bf16[8,352,128]{2,1,0:T(8,128)(2,1)} %all-to-all-done.2.refs_0_), channel_id=1, source_target_pairs={{0,1},{1,0},{2,3},{3,2},{4,5},{5,4},{6,7},{7,6},{8,9},{9,8},{10,11... | collective-permute-start | bytes 2162696 | tf_op jit(solution)/shard_map/ppermute | solution.py:196
  114.4 41.3 %collective-permute-start.9 = (bf16[8,352,128]{2,1,0:T(8,128)(2,1)}, bf16[8,352,128]{2,1,0:T(8,128)(2,1)}, u32[]{:S(2)}, u32[]{:S(2)}) collective-permute-start(bf16[8,352,128]{2,1,0:T(8,128)(2,1)} %all-to-all-done.3.refs_2_), channel_id=1, source_target_pairs={{0,4},{2,6},{4,0},{6,2},{8,12},{10,14},{12,8},{14,10},{16,20},{18,... | collective-permute-start | bytes 2162696 | tf_op jit(solution)/shard_map/ppermute | solution.py:187
  125.6 31.6 %collective-permute-start.14 = (bf16[8,352,128]{2,1,0:T(8,128)(2,1)}, bf16[8,352,128]{2,1,0:T(8,128)(2,1)}, u32[]{:S(2)}, u32[]{:S(2)}) collective-permute-start(bf16[8,352,128]{2,1,0:T(8,128)(2,1)} %all-to-all-done.3.refs_2_), channel_id=1, source_target_pairs={{0,1},{1,0},{2,3},{3,2},{4,5},{5,4},{6,7},{7,6},{8,9},{9,8},{10,11... | collective-permute-start | bytes 2162696 | tf_op jit(solution)/shard_map/ppermute | solution.py:196
  148.4 19.2 %collective-permute-start.17 = (bf16[8,352,128]{2,1,0:T(8,128)(2,1)}, bf16[8,352,128]{2,1,0:T(8,128)(2,1)S(1)}, u32[]{:S(2)}, u32[]{:S(2)}) collective-permute-start(bf16[8,352,128]{2,1,0:T(8,128)(2,1)} %all-to-all-done.4.refs_2_), channel_id=1, source_target_pairs={{0,4},{2,6},{4,0},{6,2},{8,12},{10,14},{12,8},{14,10},{16,20},{18,... | collective-permute-start | bytes 2162696 | tf_op jit(solution)/shard_map/ppermute | solution.py:187
  149.6 19.2 %collective-permute-start.18 = (bf16[8,352,128]{2,1,0:T(8,128)(2,1)}, bf16[8,352,128]{2,1,0:T(8,128)(2,1)S(1)}, u32[]{:S(2)}, u32[]{:S(2)}) collective-permute-start(bf16[8,352,128]{2,1,0:T(8,128)(2,1)} %all-to-all-done.4.refs_2_), channel_id=1, source_target_pairs={{0,1},{1,0},{2,3},{3,2},{4,5},{5,4},{6,7},{7,6},{8,9},{9,8},{10,11... | collective-permute-start | bytes 2162696 | tf_op jit(solution)/shard_map/ppermute | solution.py:196
  153.7 38.1 %collective-permute-start.7 = (bf16[288,2048]{1,0:T(8,128)(2,1)}, bf16[288,2048]{1,0:T(8,128)(2,1)S(1)}, u32[]{:S(2)}, u32[]{:S(2)}) collective-permute-start(bf16[288,2048]{1,0:T(8,128)(2,1)} %get-tuple-element.20), channel_id=1, source_target_pairs={{0,2},{2,0},{4,6},{6,4},{8,10},{10,8},{12,14},{14,12},{16,18},{18,... | collective-permute-start | bytes 3538952 | tf_op jit(solution)/shard_map/ppermute | solution.py:190
  155.7 20.8 %collective-permute-start.13 = (bf16[4,352,128]{2,1,0:T(8,128)(2,1)S(1)}, bf16[4,352,128]{2,1,0:T(8,128)(2,1)S(1)}, u32[]{:S(2)}, u32[]{:S(2)}) collective-permute-start(bf16[4,352,128]{2,1,0:T(8,128)(2,1)S(1)} %slice.100), channel_id=1, source_target_pairs={{0,1},{1,0},{2,3},{3,2},{4,5},{5,4},{6,7},{7,6},{8,9},{9,8},{10,11... | collective-permute-start | bytes 1081352 | tf_op jit(solution)/shard_map/ppermute | solution.py:196
  157.2 19.9 %collective-permute-start.12 = (bf16[4,352,128]{2,1,0:T(8,128)(2,1)S(1)}, bf16[4,352,128]{2,1,0:T(8,128)(2,1)S(1)}, u32[]{:S(2)}, u32[]{:S(2)}) collective-permute-start(bf16[4,352,128]{2,1,0:T(8,128)(2,1)S(1)} %slice.99), channel_id=1, source_target_pairs={{0,4},{2,6},{4,0},{6,2},{8,12},{10,14},{12,8},{14,10},{16,20},{18,... | collective-permute-start | bytes 1081352 | tf_op jit(solution)/shard_map/ppermute | solution.py:187
  167.6 16.6 %collective-permute-start.16 = (bf16[4,352,128]{2,1,0:T(8,128)(2,1)S(1)}, bf16[4,352,128]{2,1,0:T(8,128)(2,1)S(1)}, u32[]{:S(2)}, u32[]{:S(2)}) collective-permute-start(bf16[4,352,128]{2,1,0:T(8,128)(2,1)S(1)} %slice.102), channel_id=1, source_target_pairs={{0,1},{1,0},{2,3},{3,2},{4,5},{5,4},{6,7},{7,6},{8,9},{9,8},{10,11... | collective-permute-start | bytes 1081352 | tf_op jit(solution)/shard_map/ppermute | solution.py:196
  168.8 15.4 %collective-permute-start.15 = (bf16[4,352,128]{2,1,0:T(8,128)(2,1)S(1)}, bf16[4,352,128]{2,1,0:T(8,128)(2,1)S(1)}, u32[]{:S(2)}, u32[]{:S(2)}) collective-permute-start(bf16[4,352,128]{2,1,0:T(8,128)(2,1)S(1)} %slice.101), channel_id=1, source_target_pairs={{0,4},{2,6},{4,0},{6,2},{8,12},{10,14},{12,8},{14,10},{16,20},{18,... | collective-permute-start | bytes 1081352 | tf_op jit(solution)/shard_map/ppermute | solution.py:187
  176.5 14.3 %collective-permute-start.20 = (bf16[4,352,128]{2,1,0:T(8,128)(2,1)S(1)}, bf16[4,352,128]{2,1,0:T(8,128)(2,1)S(1)}, u32[]{:S(2)}, u32[]{:S(2)}) collective-permute-start(bf16[4,352,128]{2,1,0:T(8,128)(2,1)S(1)} %slice.104), channel_id=1, source_target_pairs={{0,1},{1,0},{2,3},{3,2},{4,5},{5,4},{6,7},{7,6},{8,9},{9,8},{10,11... | collective-permute-start | bytes 1081352 | tf_op jit(solution)/shard_map/ppermute | solution.py:196
  177.1 13.7 %collective-permute-start.19 = (bf16[4,352,128]{2,1,0:T(8,128)(2,1)S(1)}, bf16[4,352,128]{2,1,0:T(8,128)(2,1)S(1)}, u32[]{:S(2)}, u32[]{:S(2)}) collective-permute-start(bf16[4,352,128]{2,1,0:T(8,128)(2,1)S(1)} %slice.103), channel_id=1, source_target_pairs={{0,4},{2,6},{4,0},{6,2},{8,12},{10,14},{12,8},{14,10},{16,20},{18,... | collective-permute-start | bytes 1081352 | tf_op jit(solution)/shard_map/ppermute | solution.py:187
  212.5 2.7 %collective-permute-start.21 = (bf16[256,2048]{1,0:T(8,128)(2,1)S(1)}, bf16[256,2048]{1,0:T(8,128)(2,1)S(1)}, u32[]{:S(2)}, u32[]{:S(2)}) collective-permute-start(bf16[256,2048]{1,0:T(8,128)(2,1)S(1)} %slice.106), channel_id=1, source_target_pairs={{0,2},{2,0},{4,6},{6,4},{8,10},{10,8},{12,14},{14,12},{16,18},{18,... | collective-permute-start | bytes 3145736 | tf_op jit(solution)/shard_map/ppermute | solution.py:190
  215.8 15.3 %collective-permute-start.24 = (bf16[64,2048]{1,0:T(8,128)(2,1)S(1)}, bf16[64,2048]{1,0:T(8,128)(2,1)S(1)}, u32[]{:S(2)}, u32[]{:S(2)}) collective-permute-start(bf16[64,2048]{1,0:T(8,128)(2,1)S(1)} %get-tuple-element.18), channel_id=1, source_target_pairs={{0,8},{2,10},{4,12},{6,14},{8,16},{10,18},{12,20},{14,22},{16,24},... | collective-permute-start | bytes 786440 | tf_op jit(solution)/shard_map/ppermute | solution.py:193
  215.9 33.3 %collective-permute-start.23 = (bf16[64,2048]{1,0:T(8,128)(2,1)S(1)}, bf16[64,2048]{1,0:T(8,128)(2,1)S(1)}, u32[]{:S(2)}, u32[]{:S(2)}) collective-permute-start(bf16[64,2048]{1,0:T(8,128)(2,1)S(1)} %get-tuple-element.19), channel_id=1, source_target_pairs={{0,16},{2,18},{4,20},{6,22},{8,24},{10,26},{12,28},{14,30},{16,0},... | collective-permute-start | bytes 786440 | tf_op jit(solution)/shard_map/ppermute | solution.py:193
  226.0 23.2 %collective-permute-start.22 = (bf16[64,2048]{1,0:T(8,128)(2,1)S(1)}, bf16[64,2048]{1,0:T(8,128)(2,1)S(1)}, u32[]{:S(2)}, u32[]{:S(2)}) collective-permute-start(bf16[64,2048]{1,0:T(8,128)(2,1)S(1)} %get-tuple-element.17), channel_id=1, source_target_pairs={{0,24},{2,26},{4,28},{6,30},{8,0},{10,2},{12,4},{14,6},{16,8},{18,... | collective-permute-start | bytes 786440 | tf_op jit(solution)/shard_map/ppermute | solution.py:193
  (14 other events, 112.4 us)
Sparse Core Ops, SparseCore 0:
  8.9 26.7 all-gather.2
